TPU v7x, 32 devices: a whole 2x2x4 slice. The times are simulated.
32 devices in a mesh: kv: 4 (over y, x), tp: 8 (over z, core).
Axes of the slice: x: 2, y: 2, z: 4, core: 2. Of those that a mesh axis runs over, the one named last changes fastest.
Arguments:
- tokens: bfloat16 [128, 4096], P(None, 'tp'), may hold values from -6 to 6
- norm_gain: float32 [4096], P('tp'), may hold values from 0.1 to 1.9
- query_weight: bfloat16 [4096, 2048], P('tp', 'kv'), may hold values from -0.09375 to 0.09375
- key_weight: bfloat16 [4096, 2048], P('tp', 'kv'), may hold values from -0.09375 to 0.09375
- value_weight: bfloat16 [4096, 2048], P('tp', 'kv'), may hold values from -0.09375 to 0.09375
- input_gate_weight: bfloat16 [4096, 16], P('tp'), may hold values from -0.09375 to 0.09375
- forget_gate_weight: bfloat16 [4096, 16], P('tp'), may hold values from -0.09375 to 0.09375
- input_gate_bias: float32 [16], P('kv'), may hold values from -2 to 2
- forget_gate_bias: float32 [16], P('kv'), may hold values from 1 to 6
- memory_state: float32 [128, 16, 128, 128], P('tp', 'kv'), may hold values from -12 to 12
- normalizer_state: float32 [128, 16, 128], P('tp', 'kv'), may hold values from -24 to 24
- stabilizer_state: float32 [128, 16], P('tp', 'kv'), may hold values from -1 to 3
- block_keys: bfloat16 [128, 16, 128, 128], P('tp', 'kv'), may hold values from -6 to 6
- block_values: bfloat16 [128, 16, 128, 128], P('tp', 'kv'), may hold values from -6 to 6
- block_input_pre: float32 [128, 16, 128], P('tp', 'kv'), may hold values from -6 to 6
- block_forget_pre: float32 [128, 16, 128], P('tp', 'kv'), may hold values from -6 to 6
- block_lengths: int32 [128], P('tp'), may hold values from 1 to 128, 6553 in all
- head_norm_gain: float32 [2048], P('kv'), may hold values from 0.1 to 1.9
- output_weight: bfloat16 [2048, 4096], P('kv', 'tp'), may hold values from -0.125 to 0.125
- mixer_norm_gain: float32 [4096], P('tp'), may hold values from 0.1 to 1.9
- gate_weight: bfloat16 [4096, 11264], P('tp', 'kv'), may hold values from -0.09375 to 0.09375
- up_weight: bfloat16 [4096, 11264], P('tp', 'kv'), may hold values from -0.09375 to 0.09375
- down_weight: bfloat16 [11264, 4096], P('kv', 'tp'), may hold values from -0.0546875 to 0.0546875
Outputs:
- layer_output: float32 [128, 4096], P(None, 'tp')
Inputs may be any that keep to these rules, and one draw needn't show every extreme that they name: `block_lengths`: some sequence has exactly 128 live positions.
All inputs are finite; a program needn't handle non-finite values. No bound on the sum of `block_lengths` on one device may be relied on, other than what follows from the above.
Results may differ from a plain program's by a relative error of at most 0.0078.
Values may be sent and summed in bfloat16 or wider, within the bound.
No kernel may reach another device: no remote copies, remote signals or barrier semaphores. Data moves between devices by JAX's collectives and lax.ppermute only.
A program may use at most 64 MiB of HBM per device.

v0:
```python
import jax
import jax.numpy as jnp
from jax import lax
from jax.sharding import PartitionSpec as P

D = 4096
epsilon = 1e-06


def memory_cell(
    queries,
    new_keys,
    new_values,
    log_input,
    log_forget,
    memory,
    normalizer,
    stabilizer,
    cached_keys,
    cached_values,
    input_pre,
    forget_pre,
    lengths,
    input_bias,
    forget_bias,
):
    positions = jnp.arange(cached_keys.shape[2])
    is_live = (positions[None, :] < lengths[:, None])[:, None, :]
    cached_input = input_pre + input_bias[None, :, None]
    cached_forget = jnp.where(
        is_live, jax.nn.log_sigmoid(forget_pre + forget_bias[None, :, None]), 0.0
    )
    after_mask = (positions[:, None] > positions[None, :]).astype(jnp.float32)
    later_forget = (
        jnp.einsum("bhu,us->bhs", cached_forget, after_mask, precision=lax.Precision.HIGHEST)
        + log_forget[..., None]
    )
    total_forget = jnp.sum(cached_forget, axis=-1) + log_forget
    exponent = jnp.where(is_live, later_forget + cached_input, -jnp.inf)
    carried = total_forget + stabilizer
    stab_max = jnp.maximum(jnp.maximum(jnp.max(exponent, axis=-1), carried), log_input)
    scores = jnp.einsum("bhd,bhsd->bhs", queries, cached_keys, preferred_element_type=jnp.float32)
    block_weight = jnp.exp(exponent - stab_max[..., None]) * scores
    block_probs = block_weight.astype(jnp.bfloat16)
    block_sum = jnp.einsum(
        "bhs,bhsd->bhd", block_probs, cached_values, preferred_element_type=jnp.float32
    )
    query_wide = queries.astype(jnp.float32)
    new_weight = jnp.exp(log_input - stab_max) * jnp.sum(
        query_wide * new_keys.astype(jnp.float32), axis=-1
    )
    state_weight = jnp.exp(carried - stab_max)
    state_sum = jnp.einsum("bhkv,bhk->bhv", memory, query_wide, precision=lax.Precision.HIGHEST)
    state_norm = jnp.sum(normalizer * query_wide, axis=-1)
    numerator = (
        block_sum
        + new_weight[..., None] * new_values.astype(jnp.float32)
        + state_weight[..., None] * state_sum
    )
    denominator = jnp.sum(block_weight, axis=-1) + new_weight + state_weight * state_norm
    return numerator / jnp.maximum(jnp.abs(denominator), 1.0)[..., None]


def head_scale(cell_out, gain):
    return (cell_out * gain.reshape(cell_out.shape[1], cell_out.shape[2])).astype(jnp.bfloat16)


def activate(gate_sum, up_sum, square_sum):
    row_scale = lax.rsqrt(square_sum / D + epsilon)[:, None]
    return (jax.nn.silu(gate_sum * row_scale) * (up_sum * row_scale)).astype(jnp.bfloat16)


def body(
    tokens,
    norm_gain,
    query_weight,
    key_weight,
    value_weight,
    input_gate_weight,
    forget_gate_weight,
    input_gate_bias,
    forget_gate_bias,
    memory_state,
    normalizer_state,
    stabilizer_state,
    block_keys,
    block_values,
    block_input_pre,
    block_forget_pre,
    block_lengths,
    head_norm_gain,
    output_weight,
    mixer_norm_gain,
    gate_weight,
    up_weight,
    down_weight,
):
    seq_rows = block_keys.shape[0]
    heads_dev = block_keys.shape[1]
    head_size = block_keys.shape[3]
    tok_wide = tokens.astype(jnp.float32)
    scaled_in = (tok_wide * norm_gain).astype(jnp.bfloat16)
    square_part = jnp.sum(tok_wide * tok_wide, axis=1)

    def partial_of(weight):
        return jnp.dot(scaled_in, weight, preferred_element_type=jnp.float32)

    query_sum, key_sum, value_sum, input_sum, forget_sum, square_sum = (
        lax.psum_scatter(partial_of(query_weight), "tp", scatter_dimension=0, tiled=True),
        lax.psum_scatter(partial_of(key_weight), "tp", scatter_dimension=0, tiled=True),
        lax.psum_scatter(partial_of(value_weight), "tp", scatter_dimension=0, tiled=True),
        lax.psum_scatter(partial_of(input_gate_weight), "tp", scatter_dimension=0, tiled=True),
        lax.psum_scatter(partial_of(forget_gate_weight), "tp", scatter_dimension=0, tiled=True),
        lax.psum_scatter(square_part, "tp", scatter_dimension=0, tiled=True),
    )
    first_scale = lax.rsqrt(square_sum / D + epsilon)[:, None]
    queries = (
        (query_sum * first_scale * head_size ** (-0.5))
        .astype(jnp.bfloat16)
        .reshape(seq_rows, heads_dev, head_size)
    )
    new_keys = (key_sum * first_scale).astype(jnp.bfloat16).reshape(seq_rows, heads_dev, head_size)
    new_values = (
        (value_sum * first_scale).astype(jnp.bfloat16).reshape(seq_rows, heads_dev, head_size)
    )
    head_start = lax.axis_index("kv") * heads_dev
    log_input = (
        lax.dynamic_slice_in_dim(input_sum * first_scale, head_start, heads_dev, 1)
        + input_gate_bias
    )
    log_forget = jax.nn.log_sigmoid(
        lax.dynamic_slice_in_dim(forget_sum * first_scale, head_start, heads_dev, 1)
        + forget_gate_bias
    )
    cell_out = memory_cell(
        queries,
        new_keys,
        new_values,
        log_input,
        log_forget,
        memory_state,
        normalizer_state,
        stabilizer_state,
        block_keys,
        block_values,
        block_input_pre,
        block_forget_pre,
        block_lengths,
        input_gate_bias,
        forget_gate_bias,
    )
    head_out = head_scale(cell_out, head_norm_gain).reshape(seq_rows, heads_dev * head_size)
    attended_part = jnp.dot(
        lax.all_gather(head_out, "tp", axis=0, tiled=True),
        output_weight,
        preferred_element_type=jnp.float32,
    )
    attended = lax.psum(attended_part, "kv")
    res_wide = tok_wide + attended
    mid_square = jnp.sum(res_wide * res_wide, axis=1)
    mid_scaled = (res_wide * mixer_norm_gain).astype(jnp.bfloat16)
    gate_part = jnp.dot(mid_scaled, gate_weight, preferred_element_type=jnp.float32)
    up_part = jnp.dot(mid_scaled, up_weight, preferred_element_type=jnp.float32)
    gate_sum, up_sum, mid_sum = lax.psum((gate_part, up_part, mid_square), "tp")
    hidden = activate(gate_sum, up_sum, mid_sum)
    down_part = jnp.dot(hidden, down_weight, preferred_element_type=jnp.float32)
    mixed = lax.psum(down_part, "kv")
    return res_wide + mixed


def solution(mesh):
    placed = (
        P(None, "tp"),
        P("tp"),
        P("tp", "kv"),
        P("tp", "kv"),
        P("tp", "kv"),
        P("tp", None),
        P("tp", None),
        P("kv"),
        P("kv"),
        P("tp", "kv", None, None),
        P("tp", "kv", None),
        P("tp", "kv"),
        P("tp", "kv", None, None),
        P("tp", "kv", None, None),
        P("tp", "kv", None),
        P("tp", "kv", None),
        P("tp"),
        P("kv"),
        P("kv", "tp"),
        P("tp"),
        P("tp", "kv"),
        P("tp", "kv"),
        P("kv", "tp"),
    )
    return jax.shard_map(body, mesh=mesh, in_specs=placed, out_specs=P(None, "tp"), check_vma=False)
```

profile of v0, /device:TPU:0, one launch (start us, length us, event | category | flops | bytes accessed | tf_op | source)
XLA Modules:
  0.0 376.3 jit_solution(17206025061885807073)
XLA Ops:
  6.6 1.9 fusion.16
  8.5 1.7 fusion.14
  10.3 2.1 fusion.12
  12.5 2.1 fusion.10
  14.6 0.9 fusion.8
  15.8 18.1 %all-reduce = f32[128]{0:T(128)S(1)} all-reduce(f32[128]{0:T(128)S(1)} %fusion.4), channel_id=3, replica_groups=mesh['kv'=4,'tp'=8] {'tp'}, use_global_device_ids=true, to_apply=%region_2.0.clone | all-reduce | flops 128 | bytes 1024
  34.6 1.3 dynamic-slice
  36.7 0.9 fusion.32
  37.7 5.3 %reduce-scatter.16.cloned.1.call-done = f32[16,16]{1,0:T(8,128)} async-done(((f32[128,16]{1,0:T(8,128)}), f32[16,16]{1,0:T(8,128)}) %reduce-scatter.16.cloned.1.call-update) | async-done | bytes 1040
  43.9 29.9 %reduce-scatter.18.cloned.1.call-done = f32[16,16]{1,0:T(8,128)} async-done(((f32[128,16]{1,0:T(8,128)}), f32[16,16]{1,0:T(8,128)}) %reduce-scatter.18.cloned.1.call-update) | async-done | bytes 1040
  74.6 1.6 fusion.34
  76.9 27.9 %reduce-scatter.10.cloned.1.call-done = f32[16,512]{1,0:T(8,128)} async-done(((f32[128,512]{1,0:T(8,128)}), f32[16,512]{1,0:T(8,128)}) %reduce-scatter.10.cloned.1.call-update) | async-done | bytes 32784 | tf_op jit(solution)/shard_map/reduce_scatter | solution.py:109
  104.9 31.1 %reduce-scatter.12.cloned.1.call-done = f32[16,512]{1,0:T(8,128)} async-done(((f32[128,512]{1,0:T(8,128)}), f32[16,512]{1,0:T(8,128)}) %reduce-scatter.12.cloned.1.call-update) | async-done | bytes 32784 | tf_op jit(solution)/shard_map/reduce_scatter | solution.py:110
  136.0 31.1 %reduce-scatter.14.cloned.1.call-done = f32[16,512]{1,0:T(8,128)} async-done(((f32[128,512]{1,0:T(8,128)}), f32[16,512]{1,0:T(8,128)}) %reduce-scatter.14.cloned.1.call-update) | async-done | bytes 32784 | tf_op jit(solution)/shard_map/reduce_scatter | solution.py:111
  167.0 1.5 fusion.25
  170.8 4.9 %fusion.36 = f32[16,4,1,128]{3,2,1,0:T(1,128)} fusion(bf16[16,4,128,1]{2,3,1,0:T(2,128)(2,1)S(1)} %reshape.54, f32[16,4,128,128]{3,2,1,0:T(8,128)} %param.32), kind=kOutput, calls=%fused_computation.61 | convolution fusion | flops 12582912 | bytes 4243456 | tf_op jit(solution)/shard_map/bhkv,bhk->bhv/dot_general | solution.py:53
  175.8 2.0 fusion.35
  178.8 1.3 copy.52
  180.1 1.3 copy.49
  181.5 1.3 copy.50
  182.8 1.4 reshape.46
  184.2 2.3 fusion.22
  186.7 14.0 %all_gather.3 = bf16[128,512]{1,0:T(8,128)(2,1)S(1)} all-gather(bf16[16,512]{1,0:T(8,128)(2,1)S(1)} %bitcast.45), channel_id=1, replica_groups=mesh['kv'=4,'tp'=8] {'tp'}, dimensions={0}, use_global_device_ids=true | all-gather | bytes 147456 | tf_op jit(solution)/shard_map/all_gather | solution.py:154
  201.7 41.3 %all-reduce.6.cloned.1.call-done = f32[128,512]{1,0:T(8,128)} async-done(((f32[128,512]{1,0:T(8,128)}), f32[128,512]{1,0:T(8,128)}) %all-reduce.6.cloned.1.call-update) | async-done | bytes 262160 | tf_op jit(solution)/shard_map/psum | solution.py:158
  243.0 1.1 multiply_reduce_fusion
  244.1 1.7 fusion.39
  246.4 1.7 fusion.38
  248.2 16.2 %psum.37 = f32[128]{0:T(128)S(1)} all-reduce(f32[128]{0:T(128)S(1)} %get-tuple-element.12), channel_id=1, replica_groups=mesh['kv'=4,'tp'=8] {'tp'}, use_global_device_ids=true, to_apply=%region_15.16 | all-reduce | flops 128 | bytes 1024 | tf_op jit(solution)/shard_map/psum | solution.py:164
  264.4 56.5 %all-reduce.10.cloned.1.call-done = (f32[128,2816]{1,0:T(8,128)}, f32[128,2816]{1,0:T(8,128)}) async-done(((f32[128,2816]{1,0:T(8,128)}, f32[128,2816]{1,0:T(8,128)}), (f32[128,2816]{1,0:T(8,128)}, f32[128,2816]{1,0:T(8,128)})) %all-reduce.10.cloned.1.call-update) | async-done | bytes 2883600 | tf_op jit(solution)/shard_map/psum | solution.py:164
  320.9 4.2 %fusion.2 = f32[128,512]{1,0:T(8,128)} fusion(bf16[2816,512]{1,0:T(8,128)(2,1)} %param.45, f32[128,2816]{1,0:T(8,128)} %get-tuple-element.7, f32[128,2816]{1,0:T(8,128)} %get-tuple-element.8, f32[128]{0:T(128)S(1)} %add_rsqrt_fusion), kind=kOutput, calls=%fused_computation.4 | convolution fusion | flops 371982336 | bytes 6029824 | tf_op jit(solution)/shard_map/dot_general | solution.py:166
  325.1 42.7 %all-reduce.8.cloned.1.call-done = f32[128,512]{1,0:T(8,128)} async-done(((f32[128,512]{1,0:T(8,128)}), f32[128,512]{1,0:T(8,128)}) %all-reduce.8.cloned.1.call-update) | async-done | bytes 262160 | tf_op jit(solution)/shard_map/psum | solution.py:167
  367.8 1.7 fusion.5
  (103 shorter events, 8.8 us)
Async XLA Ops:
  6.5 237.5 %copy-start = (bf16[512,2816]{1,0:T(8,128)(2,1)S(1)}, bf16[512,2816]{1,0:T(8,128)(2,1)}, u32[]{:S(2)}) copy-start(bf16[512,2816]{1,0:T(8,128)(2,1)} %param.44) | copy-start | bytes 8650756
  6.5 8.1 %copy-start.1 = (bf16[128,512]{1,0:T(8,128)(2,1)S(1)}, bf16[128,512]{1,0:T(8,128)(2,1)}, u32[]{:S(2)}) copy-start(bf16[128,512]{1,0:T(8,128)(2,1)} %param.23) | copy-start | bytes 393220
  6.5 8.1 %copy-start.10 = (f32[512]{0:T(512)S(1)}, f32[512]{0:T(512)}, u32[]{:S(2)}) copy-start(f32[512]{0:T(512)} %param.24) | copy-start | bytes 6148
  6.5 8.1 %copy-start.5 = (bf16[512,512]{1,0:T(8,128)(2,1)S(1)}, bf16[512,512]{1,0:T(8,128)(2,1)}, u32[]{:S(2)}) copy-start(bf16[512,512]{1,0:T(8,128)(2,1)} %param.27) | copy-start | bytes 1572868
  6.5 36.4 %reduce-scatter.16.cloned.1.call-start = ((), (), s32[]{:S(2)}) async-start(), calls=%async_computation.10 | async-start | bytes 73728
  8.5 28.2 %copy-start.22 = (f32[4]{0:T(128)S(1)}, f32[4]{0:T(128)}, u32[]{:S(2)}) copy-start(f32[4]{0:T(128)} %param.31) | copy-start | bytes 52
  8.5 66.2 %copy-start.31 = (f32[4]{0:T(128)S(1)}, f32[4]{0:T(128)}, u32[]{:S(2)}) copy-start(f32[4]{0:T(128)} %param.30) | copy-start | bytes 52
  8.5 65.3 %reduce-scatter.18.cloned.1.call-start = ((), (), s32[]{:S(2)}) async-start(), calls=%async_computation.11 | async-start | bytes 73728
  10.2 66.0 %copy-start.26 = (f32[16,4]{0,1:T(4,128)S(1)}, f32[16,4]{0,1:T(4,128)}, u32[]{:S(2)}) copy-start(f32[16,4]{0,1:T(4,128)} %param.34) | copy-start | bytes 772
  10.3 94.6 %reduce-scatter.10.cloned.1.call-start = ((), (), s32[]{:S(2)}) async-start(), calls=%async_computation.5 | async-start | bytes 294912 | tf_op jit(solution)/shard_map/reduce_scatter | solution.py:109
  12.4 123.5 %reduce-scatter.12.cloned.1.call-start = ((), (), s32[]{:S(2)}) async-start(), calls=%async_computation.6 | async-start | bytes 294912 | tf_op jit(solution)/shard_map/reduce_scatter | solution.py:110
  14.6 152.5 %reduce-scatter.14.cloned.1.call-start = ((), (), s32[]{:S(2)}) async-start(), calls=%async_computation.7 | async-start | bytes 294912 | tf_op jit(solution)/shard_map/reduce_scatter | solution.py:111
  15.6 227.4 %all-reduce.6.cloned.1.call-start = ((), (), s32[]{:S(2)}) async-start(), calls=%async_computation.8 | async-start | bytes 524288 | tf_op jit(solution)/shard_map/psum | solution.py:158
  36.7 131.8 %copy-start.24 = (f32[16]{0:T(128)}, f32[16]{0:T(128)S(1)}, u32[]{:S(2)}) copy-start(f32[16]{0:T(128)S(1)} %fusion.30) | copy-start | bytes 196
  37.6 130.9 %copy-start.17 = (f32[16,4]{0,1:T(4,128)}, f32[16,4]{0,1:T(4,128)S(1)}, u32[]{:S(2)}) copy-start(f32[16,4]{0,1:T(4,128)S(1)} %fusion.32) | copy-start | bytes 772
  43.8 124.7 %copy-start.14 = (f32[16,4]{0,1:T(4,128)}, f32[16,4]{0,1:T(4,128)S(1)}, u32[]{:S(2)}) copy-start(f32[16,4]{0,1:T(4,128)S(1)} %copy.64) | copy-start | bytes 772
  74.6 93.9 %copy-start.19 = (f32[16,4]{0,1:T(4,128)}, f32[16,4]{0,1:T(4,128)S(1)}, u32[]{:S(2)}) copy-start(f32[16,4]{0,1:T(4,128)S(1)} %copy.65) | copy-start | bytes 772
  170.8 4.9 %copy-start.3 = (bf16[16,4,128,128]{3,2,1,0:T(8,128)(2,1)S(1)}, bf16[16,4,128,128]{3,2,1,0:T(8,128)(2,1)}, u32[]{:S(2)}) copy-start(bf16[16,4,128,128]{3,2,1,0:T(8,128)(2,1)} %param.35) | copy-start | bytes 6291460
  175.7 2.3 copy-start.15
  175.7 2.3 copy-start.18
  175.7 2.3 copy-start.20
  175.8 24.9 %copy-start.6 = (bf16[512,512]{1,0:T(8,128)(2,1)S(1)}, bf16[512,512]{1,0:T(8,128)(2,1)}, u32[]{:S(2)}) copy-start(bf16[512,512]{1,0:T(8,128)(2,1)} %param.41) | copy-start | bytes 1572868
  184.2 2.3 copy-start.8
  184.2 2.3 copy-start.9
  184.2 2.3 copy-start.11
  184.2 2.3 copy-start.12
  184.2 2.3 copy-start.13
  184.2 2.3 copy-start.30
  201.6 119.3 %all-reduce.10.cloned.1.call-start = ((), (), s32[]{:S(2)}) async-start(), calls=%async_computation.12 | async-start | bytes 5767168 | tf_op jit(solution)/shard_map/psum | solution.py:164
  244.0 2.3 copy-start.2
  248.1 119.7 %all-reduce.8.cloned.1.call-start = ((), (), s32[]{:S(2)}) async-start(), calls=%async_computation.9 | async-start | bytes 524288 | tf_op jit(solution)/shard_map/psum | solution.py:167
  320.9 46.9 %copy-start.4 = (f32[128,512]{1,0:T(8,128)S(1)}, f32[128,512]{1,0:T(8,128)}, u32[]{:S(2)}) copy-start(f32[128,512]{1,0:T(8,128)} %all-reduce.6.cloned.1.call-done) | copy-start | bytes 786436
  (9 other events, 20.1 us)
Sparse Core Ops, SparseCore 0:
  9.6 33.3 reduce-scatter.15
  45.2 28.5 reduce-scatter.17
  76.0 28.8 reduce-scatter.9
  107.0 28.9 reduce-scatter.11
  138.0 28.9 reduce-scatter.13
  201.8 41.1 all-reduce.5
  248.2 72.6 all-reduce.9
  325.2 42.5 all-reduce.7
where the time goes:
time: 377 us; the launch traced here: 376 us
  waiting for transfers between devices  266 us (71%)
  blocking collectives  48.3 us (13%)
  matrix products  28 us (7%)
  between operations  14.5 us (4%)
  local copies, waits for them, and re-layouts  10.6 us (3%)
  other arithmetic  8.77 us (2%)
    psum x1, waiting for transfers between devices, body(): gate_sum, up_sum, mid_sum = lax.psum((gate_part, up_part, mid_square), 'tp')  56.5 us
    psum x1, waiting for transfers between devices, body(): mixed = lax.psum(down_part, 'kv')  42.7 us
    psum x1, waiting for transfers between devices, body(): attended = lax.psum(attended_part, 'kv')  41.3 us
    unnamed x10, waiting for transfers between devices  35.3 us
    reduce_scatter x1, waiting for transfers between devices, body(): lax.psum_scatter(partial_of(key_weight), 'tp', scatter_dimension=0, tiled...  31.1 us
    reduce_scatter x1, waiting for transfers between devices, body(): lax.psum_scatter(partial_of(value_weight), 'tp', scatter_dimension=0, til...  31.1 us
    reduce_scatter x1, waiting for transfers between devices, body(): lax.psum_scatter(partial_of(query_weight), 'tp', scatter_dimension=0, til...  27.9 us
    unnamed x1, blocking collectives  18.1 us
  transfers between devices with their start and end apart: 8, of which 8 were waited for; matrix products, arithmetic and copies ran while one was open for 4% of the time, Pallas kernels for 0%

commit v1 on v0

--- a/solution.py
+++ b/solution.py
@@ -5,6 +5,17 @@
 
 D = 4096
 epsilon = 1e-06
+
+
+def map_inputs(chunk, which_axis):
+    nd = lax.psum(1, which_axis)
+    part_now = chunk
+    for t in [
+        [(ix, ix ^ hop_no) for ix in range(nd)] for hop_no in (1, 2, 4, 8, 16) if hop_no < nd
+    ]:
+        step_out = lax.ppermute(part_now, which_axis, t)
+        part_now = part_now + step_out
+    return part_now
 
 
 def memory_cell(
@@ -164,7 +175,7 @@
     gate_sum, up_sum, mid_sum = lax.psum((gate_part, up_part, mid_square), "tp")
     hidden = activate(gate_sum, up_sum, mid_sum)
     down_part = jnp.dot(hidden, down_weight, preferred_element_type=jnp.float32)
-    mixed = lax.psum(down_part, "kv")
+    mixed = map_inputs(down_part, "kv")
     return res_wide + mixed
 
 

time: 377 us -> 346 us (0.918)
  waiting for transfers between devices: 266 us -> 234 us
    psum x1 -> x0, waiting for transfers between devices: 42.7 us -> none  [body(): mixed = lax.psum(down_part, 'kv')]
    ppermute x0 -> x2, waiting for transfers between devices: none -> 10.4 us  [map_inputs(): step_out = lax.ppermute(part_now, which_axis, t)]
    unnamed x10 -> x9, waiting for transfers between devices: 35.3 us -> 35.5 us
  transfers between devices with their start and end apart: 8 -> 9, of which waited for: 8 -> 9; matrix products, arithmetic and copies ran while one was open for 4% -> 4% of each run, Pallas kernels for 0% -> 0%
where the time goes in v1:
time: 346 us
  waiting for transfers between devices  234 us (68%)
  blocking collectives  48.4 us (14%)
  matrix products  27.2 us (8%)
  between operations  14.4 us (4%)
  local copies, waits for them, and re-layouts  10.5 us (3%)
  other arithmetic  7.87 us (2%)
    psum x1, waiting for transfers between devices, body(): gate_sum, up_sum, mid_sum = lax.psum((gate_part, up_part, mid_square), 'tp')  56.5 us
    psum x1, waiting for transfers between devices, body(): attended = lax.psum(attended_part, 'kv')  41.3 us
    unnamed x9, waiting for transfers between devices  35.5 us
    reduce_scatter x1, waiting for transfers between devices, body(): lax.psum_scatter(partial_of(value_weight), 'tp', scatter_dimension=0, til...  31.1 us
    reduce_scatter x1, waiting for transfers between devices, body(): lax.psum_scatter(partial_of(key_weight), 'tp', scatter_dimension=0, tiled...  31 us
    reduce_scatter x1, waiting for transfers between devices, body(): lax.psum_scatter(partial_of(query_weight), 'tp', scatter_dimension=0, til...  28 us
    unnamed x1, blocking collectives  18.1 us
    psum x1, blocking collectives, body(): gate_sum, up_sum, mid_sum = lax.psum((gate_part, up_part, mid_square), 'tp')  16.3 us
  transfers between devices with their start and end apart: 9, of which 9 were waited for; matrix products, arithmetic and copies ran while one was open for 4% of the time, Pallas kernels for 0%

profile of v1, /device:TPU:0, one launch (start us, length us, event | category | flops | bytes accessed | tf_op | source)
XLA Modules:
  0.0 345.5 jit_solution(9697295924172435305)
XLA Ops:
  6.6 1.9 fusion.15
  8.5 1.7 fusion.13
  10.3 2.1 fusion.11
  12.5 2.1 fusion.9
  15.8 18.1 %all-reduce = f32[128]{0:T(128)S(1)} all-reduce(f32[128]{0:T(128)S(1)} %fusion.4), channel_id=3, replica_groups=mesh['kv'=4,'tp'=8] {'tp'}, use_global_device_ids=true, to_apply=%region_2.0.clone | all-reduce | flops 128 | bytes 1024
  34.6 1.2 dynamic-slice
  37.4 5.5 %reduce-scatter.16.cloned.1.call-done = f32[16,16]{1,0:T(8,128)} async-done(((f32[128,16]{1,0:T(8,128)}), f32[16,16]{1,0:T(8,128)}) %reduce-scatter.16.cloned.1.call-update) | async-done | bytes 1040
  43.9 29.9 %reduce-scatter.18.cloned.1.call-done = f32[16,16]{1,0:T(8,128)} async-done(((f32[128,16]{1,0:T(8,128)}), f32[16,16]{1,0:T(8,128)}) %reduce-scatter.18.cloned.1.call-update) | async-done | bytes 1040
  74.6 1.6 fusion.33
  76.9 28.0 %reduce-scatter.10.cloned.1.call-done = f32[16,512]{1,0:T(8,128)} async-done(((f32[128,512]{1,0:T(8,128)}), f32[16,512]{1,0:T(8,128)}) %reduce-scatter.10.cloned.1.call-update) | async-done | bytes 32784 | tf_op jit(solution)/shard_map/reduce_scatter | solution.py:120
  104.9 31.0 %reduce-scatter.12.cloned.1.call-done = f32[16,512]{1,0:T(8,128)} async-done(((f32[128,512]{1,0:T(8,128)}), f32[16,512]{1,0:T(8,128)}) %reduce-scatter.12.cloned.1.call-update) | async-done | bytes 32784 | tf_op jit(solution)/shard_map/reduce_scatter | solution.py:121
  135.9 31.1 %reduce-scatter.14.cloned.1.call-done = f32[16,512]{1,0:T(8,128)} async-done(((f32[128,512]{1,0:T(8,128)}), f32[16,512]{1,0:T(8,128)}) %reduce-scatter.14.cloned.1.call-update) | async-done | bytes 32784 | tf_op jit(solution)/shard_map/reduce_scatter | solution.py:122
  167.0 1.5 fusion.24
  170.8 4.9 %fusion.35 = f32[16,4,1,128]{3,2,1,0:T(1,128)} fusion(bf16[16,4,128,1]{2,3,1,0:T(2,128)(2,1)S(1)} %reshape.54, f32[16,4,128,128]{3,2,1,0:T(8,128)} %param.32), kind=kOutput, calls=%fused_computation.61 | convolution fusion | flops 12582912 | bytes 4243456 | tf_op jit(solution)/shard_map/bhkv,bhk->bhv/dot_general | solution.py:64
  175.8 2.0 fusion.34
  178.8 1.3 copy.52
  180.1 1.3 copy.49
  181.4 1.4 copy.50
  182.8 1.4 reshape.46
  184.2 2.3 fusion.21
  186.7 14.0 %all_gather.3 = bf16[128,512]{1,0:T(8,128)(2,1)S(1)} all-gather(bf16[16,512]{1,0:T(8,128)(2,1)S(1)} %bitcast.45), channel_id=1, replica_groups=mesh['kv'=4,'tp'=8] {'tp'}, dimensions={0}, use_global_device_ids=true | all-gather | bytes 147456 | tf_op jit(solution)/shard_map/all_gather | solution.py:165
  201.7 41.3 %all-reduce.5.cloned.1.call-done = f32[128,512]{1,0:T(8,128)} async-done(((f32[128,512]{1,0:T(8,128)}), f32[128,512]{1,0:T(8,128)}) %all-reduce.5.cloned.1.call-update) | async-done | bytes 262160 | tf_op jit(solution)/shard_map/psum | solution.py:169
  243.0 1.1 multiply_reduce_fusion
  244.1 1.7 fusion.38
  246.4 1.7 fusion.37
  248.1 16.3 %psum.30 = f32[128]{0:T(128)S(1)} all-reduce(f32[128]{0:T(128)S(1)} %get-tuple-element.12), channel_id=1, replica_groups=mesh['kv'=4,'tp'=8] {'tp'}, use_global_device_ids=true, to_apply=%region_15.16 | all-reduce | flops 128 | bytes 1024 | tf_op jit(solution)/shard_map/psum | solution.py:175
  264.4 56.5 %all-reduce.7.cloned.1.call-done = (f32[128,2816]{1,0:T(8,128)}, f32[128,2816]{1,0:T(8,128)}) async-done(((f32[128,2816]{1,0:T(8,128)}, f32[128,2816]{1,0:T(8,128)}), (f32[128,2816]{1,0:T(8,128)}, f32[128,2816]{1,0:T(8,128)})) %all-reduce.7.cloned.1.call-update) | async-done | bytes 2883600 | tf_op jit(solution)/shard_map/psum | solution.py:175
  320.9 3.4 fusion.2
  324.4 1.5 collective-permute-start
  325.9 5.5 %collective-permute-done = f32[128,512]{1,0:T(8,128)S(1)} collective-permute-done((f32[128,512]{1,0:T(8,128)S(1)}, f32[128,512]{1,0:T(8,128)S(1)}, u32[]{:S(2)}, u32[]{:S(2)}) %collective-permute-start) | collective-permute-done | bytes 262176 | tf_op jit(solution)/shard_map/ppermute | solution.py:16
  331.5 1.5 collective-permute-start.1
  333.0 4.9 %collective-permute-done.1 = f32[128,512]{1,0:T(8,128)S(1)} collective-permute-done((f32[128,512]{1,0:T(8,128)S(1)}, f32[128,512]{1,0:T(8,128)S(1)}, u32[]{:S(2)}, u32[]{:S(2)}) %collective-permute-start.1) | collective-permute-done | bytes 262176 | tf_op jit(solution)/shard_map/ppermute | solution.py:16
  (105 shorter events, 11.4 us)
Async XLA Ops:
  6.5 237.5 %copy-start = (bf16[512,2816]{1,0:T(8,128)(2,1)S(1)}, bf16[512,2816]{1,0:T(8,128)(2,1)}, u32[]{:S(2)}) copy-start(bf16[512,2816]{1,0:T(8,128)(2,1)} %param.44) | copy-start | bytes 8650756
  6.5 8.1 %copy-start.1 = (bf16[128,512]{1,0:T(8,128)(2,1)S(1)}, bf16[128,512]{1,0:T(8,128)(2,1)}, u32[]{:S(2)}) copy-start(bf16[128,512]{1,0:T(8,128)(2,1)} %param.23) | copy-start | bytes 393220
  6.5 8.1 %copy-start.10 = (f32[512]{0:T(512)S(1)}, f32[512]{0:T(512)}, u32[]{:S(2)}) copy-start(f32[512]{0:T(512)} %param.24) | copy-start | bytes 6148
  6.5 8.1 %copy-start.5 = (bf16[512,512]{1,0:T(8,128)(2,1)S(1)}, bf16[512,512]{1,0:T(8,128)(2,1)}, u32[]{:S(2)}) copy-start(bf16[512,512]{1,0:T(8,128)(2,1)} %param.27) | copy-start | bytes 1572868
  6.5 36.4 %reduce-scatter.16.cloned.1.call-start = ((), (), s32[]{:S(2)}) async-start(), calls=%async_computation.9 | async-start | bytes 73728
  8.4 28.0 %copy-start.22 = (f32[4]{0:T(128)S(1)}, f32[4]{0:T(128)}, u32[]{:S(2)}) copy-start(f32[4]{0:T(128)} %param.31) | copy-start | bytes 52
  8.5 66.2 %copy-start.31 = (f32[4]{0:T(128)S(1)}, f32[4]{0:T(128)}, u32[]{:S(2)}) copy-start(f32[4]{0:T(128)} %param.30) | copy-start | bytes 52
  8.5 65.3 %reduce-scatter.18.cloned.1.call-start = ((), (), s32[]{:S(2)}) async-start(), calls=%async_computation.10 | async-start | bytes 73728
  10.2 66.0 %copy-start.26 = (f32[16,4]{0,1:T(4,128)S(1)}, f32[16,4]{0,1:T(4,128)}, u32[]{:S(2)}) copy-start(f32[16,4]{0,1:T(4,128)} %param.34) | copy-start | bytes 772
  10.3 94.6 %reduce-scatter.10.cloned.1.call-start = ((), (), s32[]{:S(2)}) async-start(), calls=%async_computation.5 | async-start | bytes 294912 | tf_op jit(solution)/shard_map/reduce_scatter | solution.py:120
  12.4 123.5 %reduce-scatter.12.cloned.1.call-start = ((), (), s32[]{:S(2)}) async-start(), calls=%async_computation.6 | async-start | bytes 294912 | tf_op jit(solution)/shard_map/reduce_scatter | solution.py:121
  14.5 152.5 %reduce-scatter.14.cloned.1.call-start = ((), (), s32[]{:S(2)}) async-start(), calls=%async_computation.7 | async-start | bytes 294912 | tf_op jit(solution)/shard_map/reduce_scatter | solution.py:122
  15.6 227.4 %all-reduce.5.cloned.1.call-start = ((), (), s32[]{:S(2)}) async-start(), calls=%async_computation.8 | async-start | bytes 524288 | tf_op jit(solution)/shard_map/psum | solution.py:169
  36.5 132.0 %copy-start.24 = (f32[16]{0:T(128)}, f32[16]{0:T(128)S(1)}, u32[]{:S(2)}) copy-start(f32[16]{0:T(128)S(1)} %fusion.29) | copy-start | bytes 196
  37.4 131.1 %copy-start.17 = (f32[16,4]{0,1:T(4,128)}, f32[16,4]{0,1:T(4,128)S(1)}, u32[]{:S(2)}) copy-start(f32[16,4]{0,1:T(4,128)S(1)} %fusion.31) | copy-start | bytes 772
  43.8 124.7 %copy-start.14 = (f32[16,4]{0,1:T(4,128)}, f32[16,4]{0,1:T(4,128)S(1)}, u32[]{:S(2)}) copy-start(f32[16,4]{0,1:T(4,128)S(1)} %copy.64) | copy-start | bytes 772
  74.6 93.9 %copy-start.19 = (f32[16,4]{0,1:T(4,128)}, f32[16,4]{0,1:T(4,128)S(1)}, u32[]{:S(2)}) copy-start(f32[16,4]{0,1:T(4,128)S(1)} %copy.65) | copy-start | bytes 772
  170.8 4.9 %copy-start.3 = (bf16[16,4,128,128]{3,2,1,0:T(8,128)(2,1)S(1)}, bf16[16,4,128,128]{3,2,1,0:T(8,128)(2,1)}, u32[]{:S(2)}) copy-start(bf16[16,4,128,128]{3,2,1,0:T(8,128)(2,1)} %param.35) | copy-start | bytes 6291460
  175.7 2.3 copy-start.15
  175.7 2.3 copy-start.18
  175.8 24.9 %copy-start.6 = (bf16[512,512]{1,0:T(8,128)(2,1)S(1)}, bf16[512,512]{1,0:T(8,128)(2,1)}, u32[]{:S(2)}) copy-start(bf16[512,512]{1,0:T(8,128)(2,1)} %param.41) | copy-start | bytes 1572868
  184.2 2.3 copy-start.8
  184.2 2.3 copy-start.9
  184.2 2.3 copy-start.11
  184.2 2.3 copy-start.12
  184.2 2.3 copy-start.13
  184.2 2.3 copy-start.30
  201.6 119.3 %all-reduce.7.cloned.1.call-start = ((), (), s32[]{:S(2)}) async-start(), calls=%async_computation.11 | async-start | bytes 5767168 | tf_op jit(solution)/shard_map/psum | solution.py:175
  244.1 2.3 copy-start.2
  320.9 17.0 %copy-start.4 = (f32[128,512]{1,0:T(8,128)S(1)}, f32[128,512]{1,0:T(8,128)}, u32[]{:S(2)}) copy-start(f32[128,512]{1,0:T(8,128)} %all-reduce.5.cloned.1.call-done) | copy-start | bytes 786436
  324.4 7.1 %collective-permute-start = (f32[128,512]{1,0:T(8,128)S(1)}, f32[128,512]{1,0:T(8,128)S(1)}, u32[]{:S(2)}, u32[]{:S(2)}) collective-permute-start(f32[128,512]{1,0:T(8,128)S(1)} %fusion.2), channel_id=1, source_target_pairs={{0,8},{8,0},{16,24},{24,16},{1,9},{9,1},{17,25},{25,17},{2,10},{10... | collective-permute-start | bytes 786440 | tf_op jit(solution)/shard_map/ppermute | solution.py:16
  331.5 6.4 %collective-permute-start.1 = (f32[128,512]{1,0:T(8,128)S(1)}, f32[128,512]{1,0:T(8,128)S(1)}, u32[]{:S(2)}, u32[]{:S(2)}) collective-permute-start(f32[128,512]{1,0:T(8,128)S(1)} %add.145), channel_id=1, source_target_pairs={{0,16},{8,24},{16,0},{24,8},{1,17},{9,25},{17,1},{25,9},{2,18},{10... | collective-permute-start | bytes 786440 | tf_op jit(solution)/shard_map/ppermute | solution.py:16
  (10 other events, 22.4 us)
Sparse Core Ops, SparseCore 0:
  9.6 33.3 reduce-scatter.15
  45.2 28.5 reduce-scatter.17
  76.0 28.8 reduce-scatter.9
  107.0 28.8 reduce-scatter.11
  138.0 28.9 reduce-scatter.13
  201.7 41.2 all-reduce.4
  248.2 72.6 all-reduce.6
